TPU v7x, 32 devices: a whole 2x2x4 slice. The times are simulated.
32 devices in a mesh: sp: 8 (over z, y), tp: 4 (over x, core).
Axes of the slice: x: 2, y: 2, z: 4, core: 2. Of those that a mesh axis runs over, the one named last changes fastest.
Arguments:
- queries: bfloat16 [1024, 2048], P('sp', 'tp'), may hold values from -6 to 6
- keys: bfloat16 [1024, 512], P('sp', 'tp'), may hold values from -6 to 6
- values: bfloat16 [1024, 512], P('sp', 'tp'), may hold values from -6 to 6
- query_gain: float32 [128], replicated, may hold values from 0.3 to 7
- key_norm_gain: float32 [128], replicated, may hold values from 0.3 to 7
- out_weight: bfloat16 [2048, 2048], P('tp'), may hold values from -0.25 to 0.25
- residual: bfloat16 [1024, 2048], P(('sp', 'tp')), may hold values from -6 to 6
- norm_gain: float32 [2048], replicated, may hold values from 0.1 to 1.9
- expert_gate: bfloat16 [8, 2048, 3072], P('sp', None, 'tp'), may hold values from -0.125 to 0.125
- expert_up: bfloat16 [8, 2048, 3072], P('sp', None, 'tp'), may hold values from -0.125 to 0.125
- expert_down: bfloat16 [8, 3072, 2048], P('sp', 'tp'), may hold values from -0.109375 to 0.109375
- routes: int32 [1024, 2], P(('sp', 'tp')), may hold values from 0 to 7, all different within a row; in each aligned block of 32 rows (0 to 31, 32 to 63, ...) at most 16 rows name the same one
- route_weight: float32 [1024, 2], P(('sp', 'tp')), may hold values from 0.25 to 1
Outputs:
- mixed: bfloat16 [1024, 2048], P(('sp', 'tp'))
Inputs may be any that keep to these rules, and one draw needn't show every extreme that they name: The two experts of a token differ. In each aligned block of 32 tokens (the tokens of one device), no expert is named by more than 16 routes, and in some block one expert is named by exactly 16.
All inputs are finite; a program needn't handle non-finite values.
Results may differ from a plain program's by a relative error of at most 0.013.
The roundings to bfloat16 on the way count: a program that leaves them out, or rounds other values in their place, can miss the bound.
Values may be sent and summed in bfloat16 or wider, within the bound.
A program may use at most 64 MiB of HBM per device.

v0:
```python
import functools
import math

import jax
import jax.numpy as jnp
from jax import lax
from jax.experimental import pallas as pl
from jax.experimental.pallas import tpu as pltpu
from jax.sharding import PartitionSpec as P

HEAD_SIZE = 128
GRID_W = 64


norm_eps = 1e-06
theta_base = 10000.0


def head_normalize(packed, gain, heads):
    heads_float = packed.astype(jnp.float32).reshape(packed.shape[0], heads, HEAD_SIZE)
    scaled = heads_float * lax.rsqrt(
        jnp.mean(heads_float * heads_float, axis=-1, keepdims=True) + norm_eps
    )
    return scaled * gain


def rotary_tables(positions):
    freq_count = HEAD_SIZE // 4
    grid_row = (positions // GRID_W).astype(jnp.float32)
    grid_col = (positions % GRID_W).astype(jnp.float32)
    inverse = theta_base ** (-jnp.arange(freq_count, dtype=jnp.float32) * 2.0 / (HEAD_SIZE // 2))
    by_row = grid_row[:, None] * inverse
    by_col = grid_col[:, None] * inverse
    angles = jnp.concatenate([by_row, by_row, by_col, by_col], axis=-1)
    return (jnp.cos(angles), jnp.sin(angles))


def apply_rotation(heads_float, cosine_table, sine_values):
    freq_count = HEAD_SIZE // 4
    split_head = heads_float.reshape(heads_float.shape[:-1] + (2, 2, freq_count))
    turned = jnp.stack([-split_head[..., 1, :], split_head[..., 0, :]], axis=-2).reshape(
        heads_float.shape
    )
    return heads_float * cosine_table[:, None, :] + turned * sine_values[:, None, :]


def on_device(
    queries,
    keys,
    values,
    query_gain,
    key_norm_gain,
    out_weight,
    residual,
    norm_gain,
    expert_gate,
    expert_up,
    expert_down,
    routes,
    route_weight,
):
    local_rows = queries.shape[0]
    query_heads = queries.shape[1] // HEAD_SIZE
    key_heads = keys.shape[1] // HEAD_SIZE
    group_members = query_heads // key_heads
    score_scale = 1.0 / math.sqrt(HEAD_SIZE)
    positions = lax.axis_index("sp") * local_rows + jnp.arange(local_rows, dtype=jnp.int32)
    cosine_table, sine_values = rotary_tables(positions)
    rotated_queries = apply_rotation(
        head_normalize(queries, query_gain, query_heads), cosine_table, sine_values
    ).astype(jnp.bfloat16)
    query_block = rotated_queries.reshape(
        local_rows, key_heads, group_members, HEAD_SIZE
    ).transpose(1, 2, 0, 3)
    query_block = query_block.reshape(key_heads, group_members * local_rows, HEAD_SIZE)
    rotated_keys = apply_rotation(
        head_normalize(keys, key_norm_gain, key_heads), cosine_table, sine_values
    ).astype(jnp.bfloat16)
    rotated_keys = rotated_keys.reshape(local_rows, key_heads * HEAD_SIZE)
    start_state = (
        jnp.full((key_heads, group_members * local_rows), -1e30, jnp.float32),
        jnp.zeros((key_heads, group_members * local_rows), jnp.float32),
        jnp.zeros((key_heads, group_members * local_rows, HEAD_SIZE), jnp.float32),
    )
    folded = start_state
    key_piece = lax.all_gather(rotated_keys, "sp", axis=0, tiled=True)
    value_piece = lax.all_gather(values, "sp", axis=0, tiled=True)
    key_count = key_piece.shape[0]
    span_size = 512
    key_spans = key_piece.reshape(key_count // span_size, span_size, key_heads, HEAD_SIZE)
    value_spans = value_piece.reshape(key_count // span_size, span_size, key_heads, HEAD_SIZE)

    def one_span(state, span_pair):
        running, norm_sum, gathered_sum = state
        key_span, value_span = span_pair
        scores = (
            jnp.einsum("hqd,khd->hqk", query_block, key_span, preferred_element_type=jnp.float32)
            * score_scale
        )
        newest = jnp.maximum(running, jnp.max(scores, axis=-1))
        shrink = jnp.exp(running - newest)
        weights = jnp.exp(scores - newest[..., None])
        norm_sum = norm_sum * shrink + jnp.sum(weights, axis=-1)
        gathered_sum = gathered_sum * shrink[..., None] + jnp.einsum(
            "hqk,khd->hqd",
            weights.astype(jnp.bfloat16),
            value_span,
            preferred_element_type=jnp.float32,
        )
        return ((newest, norm_sum, gathered_sum), None)

    folded, _ = lax.scan(one_span, folded, (key_spans, value_spans))
    running, norm_sum, gathered_sum = folded
    attention = (gathered_sum / norm_sum[..., None]).reshape(
        key_heads, group_members, local_rows, HEAD_SIZE
    )
    attention = (
        attention.transpose(2, 0, 1, 3)
        .reshape(local_rows, query_heads * HEAD_SIZE)
        .astype(jnp.bfloat16)
    )
    out_rows = residual.shape[0]
    model_width = residual.shape[1]
    projected = lax.psum_scatter(
        jnp.dot(attention, out_weight, preferred_element_type=jnp.float32).astype(jnp.bfloat16),
        "tp",
        scatter_dimension=0,
        tiled=True,
    ).astype(jnp.float32)
    hidden_state = residual.astype(jnp.float32) + projected
    normed = (
        hidden_state
        * lax.rsqrt(jnp.mean(hidden_state * hidden_state, axis=-1, keepdims=True) + norm_eps)
        * norm_gain
    ).astype(jnp.bfloat16)
    route_top = routes.shape[1]
    group_width = lax.axis_size("tp")
    expert_count = lax.axis_size("sp") * expert_gate.shape[0]
    capacity = 2 * max(1, route_top * local_rows // (group_width * expert_count))
    flat_routes = routes.reshape(-1)
    onehot = (flat_routes[:, None] == jnp.arange(expert_count, dtype=jnp.int32)[None, :]).astype(
        jnp.int32
    )
    earlier = jnp.cumsum(onehot, axis=0) - onehot
    slot_rank = jnp.sum(earlier * onehot, axis=1)
    slot_index = flat_routes * capacity + slot_rank
    placer = (
        jnp.arange(expert_count * capacity, dtype=jnp.int32)[:, None] == slot_index[None, :]
    ).astype(jnp.bfloat16)
    route_rows = jnp.repeat(normed, route_top, axis=0)
    buffer = jnp.dot(placer, route_rows, preferred_element_type=jnp.float32).astype(jnp.bfloat16)
    buffer = buffer.reshape(expert_count, capacity, model_width)
    mail_rows = lax.all_to_all(buffer, "sp", split_axis=0, concat_axis=0, tiled=True)
    inbox_rows = lax.all_gather(mail_rows, "tp", axis=1, tiled=True)
    source_count = inbox_rows.shape[0]
    rows_in = inbox_rows.reshape(-1, model_width)
    gate_proj = jnp.dot(rows_in, expert_gate[0], preferred_element_type=jnp.float32)
    up_proj = jnp.dot(rows_in, expert_up[0], preferred_element_type=jnp.float32)
    hidden_act = (jax.nn.silu(gate_proj) * up_proj).astype(jnp.bfloat16)
    down_part = jnp.dot(hidden_act, expert_down[0], preferred_element_type=jnp.float32)
    down_part = down_part.reshape(source_count, group_width * capacity, model_width)
    summed = lax.psum_scatter(down_part.astype(jnp.bfloat16), "tp", scatter_dimension=1, tiled=True)
    returned = lax.all_to_all(summed, "sp", split_axis=0, concat_axis=0, tiled=True)
    per_route = jnp.dot(
        placer.T, returned.reshape(-1, model_width), preferred_element_type=jnp.float32
    )
    per_route = per_route.reshape(out_rows, route_top, model_width)
    moe_sum = jnp.sum(route_weight[:, :, None] * per_route, axis=1)
    return (hidden_state + moe_sum).astype(jnp.bfloat16)


MESH = pl.DeviceIdType.MESH
LOG2E = 1.4426950408889634


def layer_kernel(
    dims,
    cos_ref,
    sina_ref,
    sinb_ref,
    k_hbm,
    kgain_hbm,
    v_hbm,
    q_hbm,
    qgain_hbm,
    wout_hbm,
    routes_hbm,
    weight_hbm,
    resid_hbm,
    ngain_hbm,
    gate_hbm,
    up_hbm,
    down_hbm,
    out_ref,
    k_ref,
    kgain_ref,
    v_ref,
    q_ref,
    qgain_ref,
    routes_ref,
    weight_ref,
    resid_ref,
    ngain_ref,
    picks,
    placed_ref,
    wcol,
    wout,
    wgate,
    wup,
    wdown,
    kv,
    att,
    part,
    rs_in,
    state,
    mail,
    inbox,
    hidden,
    keep,
    pair_out,
    pair_in,
    xsum,
    xin,
    outmail,
    back,
    wsem,
    kv_send,
    kv_fsend,
    kv_recv,
    rs_send,
    rs_recv,
    mail_send,
    x_send,
    p_send,
    f_send,
    in_recv,
    pair_send,
    pair_recv,
    rx_send,
    rx_recv,
    back_send,
    back_recv,
):
    nsp, ntp, heads, cap, rows, own_rows = dims
    width = out_ref.shape[1]
    span = nsp // 2
    me = lax.axis_index("sp")
    tp = lax.axis_index("tp")
    far = me // 2
    near = me % 2
    side = tp // 2
    core = tp % 2
    mate = side * 2 + (1 - core)
    across = (1 - side) * 2 + core
    diagonal = (1 - side) * 2 + (1 - core)
    twin = far * 2 + (1 - near)

    def flip(index, mask):
        value, bit = 0, 1
        while bit < nsp:
            digit = (index // bit) % 2
            value = value + bit * (1 - digit if mask & bit else digit)
            bit *= 2
        return value

    def peer(d):
        return flip(me, d)

    loads = []
    for i, (hbm, local) in enumerate(
        (
            (k_hbm, k_ref),
            (kgain_hbm, kgain_ref),
            (v_hbm, kv.at[me, :, pl.ds(HEAD_SIZE, HEAD_SIZE)]),
            (q_hbm, q_ref),
            (qgain_hbm, qgain_ref),
            (wout_hbm, wout),
            (routes_hbm, routes_ref),
            (weight_hbm, weight_ref),
            (resid_hbm, resid_ref),
            (ngain_hbm, ngain_ref),
            (gate_hbm.at[0], wgate),
            (up_hbm.at[0], wup),
            (down_hbm.at[0], wdown),
        )
    ):
        load = pltpu.make_async_copy(hbm, local, wsem.at[i])
        load.start()
        loads.append(load)

    barrier = pltpu.get_barrier_semaphore()
    for d in range(1, nsp):
        pl.semaphore_signal(barrier, inc=1, device_id=(peer(d), tp), device_id_type=MESH)
    for d in range(1, ntp):
        pl.semaphore_signal(
            barrier, inc=1, device_id=(me, lax.rem(tp + d, ntp)), device_id_type=MESH
        )

    sent = []

    def push(source, target, send_sem, recv_sem, to_sp, to_tp):
        copy = pltpu.make_async_remote_copy(
            src_ref=source,
            dst_ref=target,
            send_sem=send_sem,
            recv_sem=recv_sem,
            device_id=(to_sp, to_tp),
            device_id_type=MESH,
        )
        copy.start()
        sent.append(copy)

    def arrived(target, send_sem, recv_sem):
        pltpu.make_async_remote_copy(
            src_ref=target,
            dst_ref=target,
            send_sem=send_sem,
            recv_sem=recv_sem,
            device_id=(twin, tp),
            device_id_type=MESH,
        ).wait_recv()

    def turned(head, gain_ref):
        wide = head.astype(jnp.float32)
        scaled = wide * lax.rsqrt(jnp.mean(wide * wide, axis=-1, keepdims=True) + norm_eps)
        scaled = scaled * gain_ref[...]
        quarter = HEAD_SIZE // 4
        return (
            scaled * cos_ref[...]
            + pltpu.roll(scaled, HEAD_SIZE - quarter, 1) * sina_ref[...]
            + pltpu.roll(scaled, quarter, 1) * sinb_ref[...]
        ).astype(jnp.bfloat16)

    loads[0].wait()
    loads[1].wait()
    kv[me, :, :HEAD_SIZE] = turned(k_ref[...], kgain_ref)
    loads[2].wait()
    pl.semaphore_wait(barrier, nsp - 1 + ntp - 1)

    push(kv.at[me], kv.at[me], kv_send.at[0], kv_recv.at[me], twin, tp)
    for d in range(1, span):
        push(kv.at[me], kv.at[me], kv_send.at[d], kv_recv.at[me], peer(2 * d), tp)

    loads[3].wait()
    loads[4].wait()
    queries = [
        turned(q_ref[:, h * HEAD_SIZE : (h + 1) * HEAD_SIZE], qgain_ref) for h in range(heads)
    ]
    for h in range(heads):
        att[:, h * HEAD_SIZE : (h + 1) * HEAD_SIZE] = queries[h]

    loads[6].wait()
    loads[7].wait()
    which = lax.broadcasted_iota(jnp.int32, (nsp, own_rows), 0)
    named = [which == routes_ref[j : j + 1, :] for j in range(routes_ref.shape[0])]
    named = [jnp.where(hit, 1.0, 0.0) for hit in named]
    hits = functools.reduce(jnp.add, named)
    square = (own_rows, own_rows)
    one, two = (lax.broadcasted_iota(jnp.int32, square, axis) for axis in (0, 1))
    rank = jnp.dot(
        hits.astype(jnp.bfloat16),
        jnp.where(one < two, 1.0, 0.0).astype(jnp.bfloat16),
        preferred_element_type=jnp.float32,
    )
    places = lax.broadcasted_iota(jnp.int32, (nsp, cap, own_rows), 1)
    ranked = jnp.where(places == rank.astype(jnp.int32)[:, None, :], 1.0, 0.0)
    placer = (ranked * hits[:, None, :]).reshape(nsp * cap, own_rows).astype(jnp.bfloat16)
    for j, hit in enumerate(named):
        picks[j] = (ranked * hit[:, None, :]).reshape(nsp * cap, own_rows).astype(jnp.bfloat16)
        column = jnp.sum(
            jnp.where(one == two, weight_ref[j : j + 1, :], 0.0), axis=1, keepdims=True
        )
        wcol[j] = jnp.broadcast_to(column, wcol.shape[1:])
    placed_ref[...] = placer

    for d in range(1, span):
        source = peer(2 * d)
        arrived(kv.at[source], kv_send.at[0], kv_recv.at[source])
        push(kv.at[source], kv.at[source], kv_fsend.at[d], kv_recv.at[source], twin, tp)
    for d in range(span):
        source = peer(2 * d + 1)
        arrived(kv.at[source], kv_send.at[0], kv_recv.at[source])

    scale = LOG2E / math.sqrt(HEAD_SIZE)
    for h in range(heads):
        columns = slice(h * HEAD_SIZE, (h + 1) * HEAD_SIZE)
        all_keys = kv[:, :, :HEAD_SIZE].reshape(nsp * rows, HEAD_SIZE)
        scores = lax.dot_general(
            att[:, columns],
            all_keys,
            (((1,), (1,)), ((), ())),
            preferred_element_type=jnp.float32,
        )
        top = jnp.max(scores, axis=-1, keepdims=True)
        weights = jnp.exp2((scores - top) * scale)
        norm_sum = jnp.sum(weights, axis=-1, keepdims=True)
        all_values = kv[:, :, HEAD_SIZE:].reshape(nsp * rows, HEAD_SIZE)
        mixed = jnp.dot(
            weights.astype(jnp.bfloat16), all_values, preferred_element_type=jnp.float32
        )
        att[:, columns] = (mixed / norm_sum).astype(jnp.bfloat16)

    loads[5].wait()
    tile = 512

    @pl.loop(0, width // tile)
    def _(j):
        columns = pl.ds(pl.multiple_of(j * tile, tile), tile)
        product = jnp.dot(att[...], wout[:, columns], preferred_element_type=jnp.float32)
        part[:, :, columns] = product.astype(jnp.bfloat16).reshape(ntp, own_rows, tile)

    push(part.at[diagonal], rs_in.at[1], rs_send.at[1], rs_recv.at[1], me, mate)
    push(part.at[mate], rs_in.at[2], rs_send.at[2], rs_recv.at[2], me, mate)
    arrived(rs_in.at[1], rs_send.at[1], rs_recv.at[1])
    part[across] = (
        part[across].astype(jnp.float32) + rs_in[1].astype(jnp.float32)
    ).astype(jnp.bfloat16)
    push(part.at[across], rs_in.at[3], rs_send.at[3], rs_recv.at[3], me, across)
    loads[8].wait()
    loads[9].wait()
    total = resid_ref[...].astype(jnp.float32) + part[tp].astype(jnp.float32)
    for d in (2, 3):
        arrived(rs_in.at[d], rs_send.at[d], rs_recv.at[d])
        total = total + rs_in[d].astype(jnp.float32)
    state[...] = total
    normed = (
        total
        * lax.rsqrt(jnp.mean(total * total, axis=-1, keepdims=True) + norm_eps)
        * ngain_ref[...]
    ).astype(jnp.bfloat16)
    mail[...] = (
        jnp.dot(placed_ref[...], normed, preferred_element_type=jnp.float32)
        .astype(jnp.bfloat16)
        .reshape(nsp, cap, width)
    )
    half = nsp // 2
    quarter = nsp // 4
    first = [*range(quarter), *range(half, half + quarter)]
    groups = (first, [d for d in range(nsp) if d not in first])
    relay = groups[0] + groups[1]
    leaving = sorted(first, reverse=True) + sorted(groups[1], reverse=True)
    for d in leaving:
        if d:
            to = peer(d)
            push(mail.at[to], inbox.at[tp, me], mail_send.at[d], in_recv.at[tp, me], to, tp)
    inbox[tp, me] = mail[me]

    def wait_piece(owner, d):
        source = peer(d)
        arrived(inbox.at[owner, source], mail_send.at[0], in_recv.at[owner, source])

    def spread(g):
        for d in groups[g]:
            if d:
                wait_piece(tp, d)
            piece = inbox.at[tp, peer(d)]
            arrival = in_recv.at[tp, peer(d)]
            push(piece, piece, x_send.at[d], arrival, me, across)
            push(piece, piece, p_send.at[d], arrival, me, mate)

    def forward(g):
        for d in groups[g]:
            wait_piece(across, d)
            piece = inbox.at[across, peer(d)]
            arrival = in_recv.at[across, peer(d)]
            push(piece, piece, f_send.at[d], arrival, me, mate)
        for d in groups[g]:
            wait_piece(diagonal, d)

    fine = 256

    def experts(parts):
        blocks = [(owner, peer(d)) for owner, _, g in parts for d in groups[g]]
        live = len(blocks) * cap

        @pl.loop(0, wgate.shape[1] // fine)
        def _(j):
            columns = pl.ds(pl.multiple_of(j * fine, fine), fine)
            block = jnp.concatenate([inbox[owner, source] for owner, source in blocks], axis=0)
            gate = jnp.dot(block, wgate[:, columns], preferred_element_type=jnp.float32)
            up = jnp.dot(block, wup[:, columns], preferred_element_type=jnp.float32)
            hidden[:live, columns] = (gate / (1.0 + jnp.exp(-gate)) * up).astype(jnp.bfloat16)

        @pl.loop(0, width // tile)
        def _(j):
            columns = pl.ds(pl.multiple_of(j * tile, tile), tile)
            product = jnp.dot(hidden[:live], wdown[:, columns], preferred_element_type=jnp.float32)
            product = product.reshape(len(parts), half, cap, tile)
            for i, (_, target, g) in enumerate(parts):
                target[g * half : (g + 1) * half, :, columns] = product[i].astype(target.dtype)

    def hand(i, g):
        span_of = pl.ds(g * half, half)
        k = 2 * i + g
        push(
            pair_out.at[i, span_of],
            pair_in.at[i, span_of],
            pair_send.at[k],
            pair_recv.at[k],
            me,
            mate,
        )

    def take(i, g):
        span_of = pl.ds(g * half, half)
        k = 2 * i + g
        arrived(pair_in.at[i, span_of], pair_send.at[k], pair_recv.at[k])

    def cross(g):
        take(1, g)
        for d in sorted(groups[g], reverse=True):
            slot = g * half + groups[g].index(d)
            source = peer(d)
            xsum[source] = (keep[1, slot] + pair_in[1, slot].astype(jnp.float32)).astype(
                jnp.bfloat16
            )
            push(
                xsum.at[source], xin.at[source], rx_send.at[d], rx_recv.at[source], me, across
            )

    spread(0)
    for i in (10, 11, 12):
        loads[i].wait()
    for d in groups[0]:
        wait_piece(mate, d)
    experts([(tp, keep.at[0], 0), (mate, pair_out.at[0], 0)])
    hand(0, 0)
    spread(1)
    forward(0)
    experts([(diagonal, pair_out.at[1], 0), (across, keep.at[1], 0)])
    hand(1, 0)
    cross(0)
    for d in groups[1]:
        wait_piece(mate, d)
    forward(1)
    experts(
        [
            (diagonal, pair_out.at[1], 1),
            (across, keep.at[1], 1),
            (tp, keep.at[0], 1),
            (mate, pair_out.at[0], 1),
        ]
    )
    hand(1, 1)
    hand(0, 1)
    cross(1)
    for d in leaving:
        g = 0 if d in first else 1
        slot = g * half + groups[g].index(d)
        source = peer(d)
        if d == leaving[g * half]:
            take(0, g)
        arrived(xin.at[source], rx_send.at[0], rx_recv.at[source])
        summed = (
            keep[0, slot]
            + pair_in[0, slot].astype(jnp.float32)
            + xin[source].astype(jnp.float32)
        ).astype(jnp.bfloat16)
        if d:
            outmail[source] = summed
            push(
                outmail.at[source], back.at[me], back_send.at[d], back_recv.at[me], source, tp
            )
        else:
            back[me] = summed
    for d in range(1, nsp):
        source = peer(d)
        arrived(back.at[source], back_send.at[0], back_recv.at[source])
    returned = back[...].reshape(nsp * cap, width)
    result = state[...]
    for j in range(picks.shape[0]):
        chosen = lax.dot_general(
            picks[j], returned, (((0,), (0,)), ((), ())), preferred_element_type=jnp.float32
        )
        result = result + wcol[j, :, 0:1] * chosen
    out_ref[...] = result.astype(out_ref.dtype)
    for copy in sent:
        copy.wait_send()


def on_device_fused(
    queries,
    keys,
    values,
    query_gain,
    key_norm_gain,
    out_weight,
    residual,
    norm_gain,
    expert_gate,
    expert_up,
    expert_down,
    routes,
    route_weight,
):
    nsp = lax.axis_size("sp")
    ntp = lax.axis_size("tp")
    rows = queries.shape[0]
    heads = queries.shape[1] // HEAD_SIZE
    own_rows, width = residual.shape
    top = routes.shape[1]
    cap = 2 * max(1, top * rows // (ntp * nsp))
    hidden_units = expert_gate.shape[2]
    positions = lax.axis_index("sp") * rows + jnp.arange(rows, dtype=jnp.int32)
    cosine, sine = rotary_tables(positions)
    first = (jnp.arange(HEAD_SIZE) % (HEAD_SIZE // 2) < HEAD_SIZE // 4)[None, :]
    sine_a = jnp.where(first, -sine, 0.0)
    sine_b = jnp.where(first, 0.0, sine)
    vmem = pl.BlockSpec(memory_space=pltpu.VMEM)
    hbm = pl.BlockSpec(memory_space=pltpu.MemorySpace.HBM)
    half, full = jnp.bfloat16, jnp.float32
    dma = pltpu.SemaphoreType.DMA
    return pl.pallas_call(
        functools.partial(layer_kernel, (nsp, ntp, heads, cap, rows, own_rows)),
        out_shape=jax.ShapeDtypeStruct((own_rows, width), half),
        in_specs=[vmem] * 3 + [hbm] * 13,
        out_specs=vmem,
        scratch_shapes=[
            pltpu.VMEM(keys.shape, half),
            pltpu.VMEM((1, HEAD_SIZE), full),
            pltpu.VMEM(values.shape, half),
            pltpu.VMEM(queries.shape, half),
            pltpu.VMEM((1, HEAD_SIZE), full),
            pltpu.VMEM((top, own_rows), jnp.int32),
            pltpu.VMEM((top, own_rows), full),
            pltpu.VMEM((own_rows, width), half),
            pltpu.VMEM((1, width), full),
            pltpu.VMEM((top, nsp * cap, own_rows), half),
            pltpu.VMEM((nsp * cap, own_rows), half),
            pltpu.VMEM((top, own_rows, HEAD_SIZE), full),
            pltpu.VMEM(out_weight.shape, half),
            pltpu.VMEM(expert_gate.shape[1:], half),
            pltpu.VMEM(expert_up.shape[1:], half),
            pltpu.VMEM(expert_down.shape[1:], half),
            pltpu.VMEM((nsp, rows, 2 * HEAD_SIZE), half),
            pltpu.VMEM(queries.shape, half),
            pltpu.VMEM((ntp, own_rows, width), half),
            pltpu.VMEM((ntp, own_rows, width), half),
            pltpu.VMEM((own_rows, width), full),
            pltpu.VMEM((nsp, cap, width), half),
            pltpu.VMEM((ntp, nsp, cap, width), half),
            pltpu.VMEM((2 * nsp * cap, hidden_units), half),
            pltpu.VMEM((2, nsp, cap, width), full),
            pltpu.VMEM((2, nsp, cap, width), half),
            pltpu.VMEM((2, nsp, cap, width), half),
            pltpu.VMEM((nsp, cap, width), half),
            pltpu.VMEM((nsp, cap, width), half),
            pltpu.VMEM((nsp, cap, width), half),
            pltpu.VMEM((nsp, cap, width), half),
            dma((13,)),
            dma((nsp // 2,)),
            dma((nsp // 2,)),
            dma((nsp,)),
            dma((ntp,)),
            dma((ntp,)),
            dma((nsp,)),
            dma((nsp,)),
            dma((nsp,)),
            dma((nsp,)),
            dma((ntp, nsp)),
            dma((4,)),
            dma((4,)),
            dma((nsp,)),
            dma((nsp,)),
            dma((nsp,)),
            dma((nsp,)),
        ],
        compiler_params=pltpu.CompilerParams(
            collective_id=0, has_side_effects=True, vmem_limit_bytes=66_800_000
        ),
    )(
        cosine,
        sine_a,
        sine_b,
        keys,
        key_norm_gain[None, :],
        values,
        queries,
        query_gain[None, :],
        out_weight,
        routes.T,
        route_weight.T,
        residual,
        norm_gain[None, :],
        expert_gate,
        expert_up,
        expert_down,
    )


def fits_fused(mesh):
    return mesh.shape["tp"] == 4 and mesh.shape["sp"] in (4, 8)


def solution(mesh):
    body = on_device_fused if fits_fused(mesh) else on_device
    placed = (
        P("sp", "tp"),
        P("sp", "tp"),
        P("sp", "tp"),
        P(),
        P(),
        P("tp", None),
        P(("sp", "tp"), None),
        P(),
        P("sp", None, "tp"),
        P("sp", None, "tp"),
        P("sp", "tp", None),
        P(("sp", "tp"), None),
        P(("sp", "tp"), None),
    )
    return jax.shard_map(
        body, mesh=mesh, in_specs=placed, out_specs=P(("sp", "tp"), None), check_vma=False
    )
```

profile of v0, /device:TPU:0, one launch (start us, length us, event | category | flops | bytes accessed | tf_op | source)
XLA Modules:
  0.0 67.7 jit_solution(5921372143950839926)
XLA Ops:
  0.0 0.1 broadcast_multiply_fusion.1
  0.1 1.0 %broadcast_select_fusion = (f32[128,128]{1,0:T(8,128)}, f32[128,128]{1,0:T(8,128)}, f32[128,128]{1,0:T(8,128)}) fusion(pred[128]{0:T(512)(128)(4,1)S(1)} %fusion.3, f32[128,32]{1,0:T(8,128)S(1)} %get-tuple-element.9, f32[128,32]{1,0:T(8,128)S(1)} %get-tuple-element.8), kind=kLoop, calls=%fused_computation.2 | loop fusion | flops 98304 | bytes 229504 | tf_op jit(solution)/shard_map/jit(_where)/select_n | solution.py:608
  1.2 65.0 %shard_map.127 = bf16[32,2048]{1,0:T(8,128)(2,1)} custom-call(f32[128,128]{1,0:T(8,128)} %get-tuple-element.7.cos_ref, f32[128,128]{1,0:T(8,128)} %get-tuple-element.6.sina_ref, f32[128,128]{1,0:T(8,128)} %get-tuple-element.5.sinb_ref, bf16[128,128]{1,0:T(8,128)(2,1)} %k_hbm.1, f32[1,128]{1,0:T(1,128)} %bitcast.8, bf16[128,128]{1,0:T(8,128)(2,1)} %v_hbm.1, ...), custom_call_target="tpu_custom_call" | custom-call | tf_op jit(solution)/shard_map/pallas_call | solution.py:613
  66.2 1.6 %copy.15 = bf16[32,2048]{1,0:T(8,128)(2,1)} copy(bf16[32,2048]{1,0:T(8,128)(2,1)} %shard_map.127) | data formatting | bytes 262144
  (3 shorter events, 0.0 us)
where the time goes:
time: 67.9 us; the launch traced here: 67.7 us
  Pallas kernels  65 us (96%)
  local copies, waits for them, and re-layouts  1.57 us (2%)
  other arithmetic  1.14 us (2%)
    pallas_call x1, Pallas kernels, on_device_fused(): pl.pallas_call(functools.partial(layer_kernel, (nsp, ntp, heads, cap, row...  65 us
    unnamed x1, local copies, waits for them, and re-layouts  1.57 us

commit v1 on v0

--- a/solution.py
+++ b/solution.py
@@ -3,6 +3,7 @@
 
 import jax
 import jax.numpy as jnp
+import numpy as np
 from jax import lax
 from jax.experimental import pallas as pl
 from jax.experimental.pallas import tpu as pltpu
@@ -175,9 +176,8 @@
 
 def layer_kernel(
     dims,
-    cos_ref,
-    sina_ref,
-    sinb_ref,
+    row_hbm,
+    column_hbm,
     k_hbm,
     kgain_hbm,
     v_hbm,
@@ -192,6 +192,8 @@
     up_hbm,
     down_hbm,
     out_ref,
+    row_ref,
+    column_ref,
     k_ref,
     kgain_ref,
     v_ref,
@@ -271,14 +273,16 @@
         (
             (k_hbm, k_ref),
             (kgain_hbm, kgain_ref),
+            (row_hbm.at[me], row_ref),
+            (column_hbm, column_ref),
             (v_hbm, kv.at[me, :, pl.ds(HEAD_SIZE, HEAD_SIZE)]),
             (q_hbm, q_ref),
             (qgain_hbm, qgain_ref),
-            (wout_hbm, wout),
             (routes_hbm, routes_ref),
             (weight_hbm, weight_ref),
             (resid_hbm, resid_ref),
             (ngain_hbm, ngain_ref),
+            (wout_hbm, wout),
             (gate_hbm.at[0], wgate),
             (up_hbm.at[0], wup),
             (down_hbm.at[0], wdown),
@@ -320,37 +324,55 @@
             device_id_type=MESH,
         ).wait_recv()
 
-    def turned(head, gain_ref):
+    lane = lax.broadcasted_iota(jnp.int32, (1, HEAD_SIZE), 1)
+    leading = lane % (HEAD_SIZE // 2) < HEAD_SIZE // 4
+
+    def table(part):
+        lanes = slice(part * HEAD_SIZE, (part + 1) * HEAD_SIZE)
+        by_column = column_ref[:, lanes]
+        return jnp.concatenate(
+            [
+                jnp.where(lane < HEAD_SIZE // 2, row_ref[k : k + 1, lanes], by_column)
+                for k in range(row_ref.shape[0])
+            ],
+            axis=0,
+        )
+
+    def turned(head, gain_ref, tables):
+        cosine, sine_a, sine_b = tables
         wide = head.astype(jnp.float32)
         scaled = wide * lax.rsqrt(jnp.mean(wide * wide, axis=-1, keepdims=True) + norm_eps)
         scaled = scaled * gain_ref[...]
         quarter = HEAD_SIZE // 4
         return (
-            scaled * cos_ref[...]
-            + pltpu.roll(scaled, HEAD_SIZE - quarter, 1) * sina_ref[...]
-            + pltpu.roll(scaled, quarter, 1) * sinb_ref[...]
+            scaled * cosine
+            + pltpu.roll(scaled, HEAD_SIZE - quarter, 1) * sine_a
+            + pltpu.roll(scaled, quarter, 1) * sine_b
         ).astype(jnp.bfloat16)
 
-    loads[0].wait()
-    loads[1].wait()
-    kv[me, :, :HEAD_SIZE] = turned(k_ref[...], kgain_ref)
-    loads[2].wait()
+    for i in (0, 1, 2, 3):
+        loads[i].wait()
+    sine = table(1)
+    tables = (table(0), jnp.where(leading, -sine, 0.0), jnp.where(leading, 0.0, sine))
+    kv[me, :, :HEAD_SIZE] = turned(k_ref[...], kgain_ref, tables)
+    loads[4].wait()
     pl.semaphore_wait(barrier, nsp - 1 + ntp - 1)
 
     push(kv.at[me], kv.at[me], kv_send.at[0], kv_recv.at[me], twin, tp)
     for d in range(1, span):
         push(kv.at[me], kv.at[me], kv_send.at[d], kv_recv.at[me], peer(2 * d), tp)
 
-    loads[3].wait()
-    loads[4].wait()
+    loads[5].wait()
+    loads[6].wait()
     queries = [
-        turned(q_ref[:, h * HEAD_SIZE : (h + 1) * HEAD_SIZE], qgain_ref) for h in range(heads)
+        turned(q_ref[:, h * HEAD_SIZE : (h + 1) * HEAD_SIZE], qgain_ref, tables)
+        for h in range(heads)
     ]
     for h in range(heads):
         att[:, h * HEAD_SIZE : (h + 1) * HEAD_SIZE] = queries[h]
 
-    loads[6].wait()
     loads[7].wait()
+    loads[8].wait()
     which = lax.broadcasted_iota(jnp.int32, (nsp, own_rows), 0)
     named = [which == routes_ref[j : j + 1, :] for j in range(routes_ref.shape[0])]
     named = [jnp.where(hit, 1.0, 0.0) for hit in named]
@@ -400,7 +422,7 @@
         )
         att[:, columns] = (mixed / norm_sum).astype(jnp.bfloat16)
 
-    loads[5].wait()
+    loads[11].wait()
     tile = 512
 
     @pl.loop(0, width // tile)
@@ -416,8 +438,8 @@
         part[across].astype(jnp.float32) + rs_in[1].astype(jnp.float32)
     ).astype(jnp.bfloat16)
     push(part.at[across], rs_in.at[3], rs_send.at[3], rs_recv.at[3], me, across)
-    loads[8].wait()
     loads[9].wait()
+    loads[10].wait()
     total = resid_ref[...].astype(jnp.float32) + part[tp].astype(jnp.float32)
     for d in (2, 3):
         arrived(rs_in.at[d], rs_send.at[d], rs_recv.at[d])
@@ -519,7 +541,7 @@
             )
 
     spread(0)
-    for i in (10, 11, 12):
+    for i in (12, 13, 14):
         loads[i].wait()
     for d in groups[0]:
         wait_piece(mate, d)
@@ -578,6 +600,24 @@
         copy.wait_send()
 
 
+def pinned(array):
+    return pltpu.with_memory_space_constraint(jnp.asarray(array), pltpu.MemorySpace.HBM)
+
+
+def grid_tables(nsp, rows):
+    count = HEAD_SIZE // 4
+    inverse = theta_base ** (-np.arange(count, dtype=np.float64) * 2.0 / (HEAD_SIZE // 2))
+    inverse = np.tile(inverse.astype(np.float32), 4)[None, :]
+
+    def both(amount):
+        angles = np.arange(amount, dtype=np.float32)[:, None] * inverse
+        pair = [np.cos(angles), np.sin(angles)]
+        return np.concatenate(pair, axis=1).astype(np.float32)
+
+    lines = rows // GRID_W
+    return both(nsp * lines).reshape(nsp, lines, 2 * HEAD_SIZE), both(GRID_W)
+
+
 def on_device_fused(
     queries,
     keys,
@@ -601,11 +641,7 @@
     top = routes.shape[1]
     cap = 2 * max(1, top * rows // (ntp * nsp))
     hidden_units = expert_gate.shape[2]
-    positions = lax.axis_index("sp") * rows + jnp.arange(rows, dtype=jnp.int32)
-    cosine, sine = rotary_tables(positions)
-    first = (jnp.arange(HEAD_SIZE) % (HEAD_SIZE // 2) < HEAD_SIZE // 4)[None, :]
-    sine_a = jnp.where(first, -sine, 0.0)
-    sine_b = jnp.where(first, 0.0, sine)
+    by_row, by_column = grid_tables(nsp, rows)
     vmem = pl.BlockSpec(memory_space=pltpu.VMEM)
     hbm = pl.BlockSpec(memory_space=pltpu.MemorySpace.HBM)
     half, full = jnp.bfloat16, jnp.float32
@@ -613,9 +649,11 @@
     return pl.pallas_call(
         functools.partial(layer_kernel, (nsp, ntp, heads, cap, rows, own_rows)),
         out_shape=jax.ShapeDtypeStruct((own_rows, width), half),
-        in_specs=[vmem] * 3 + [hbm] * 13,
+        in_specs=[hbm] * 15,
         out_specs=vmem,
         scratch_shapes=[
+            pltpu.VMEM(by_row.shape[1:], full),
+            pltpu.VMEM(by_column.shape, full),
             pltpu.VMEM(keys.shape, half),
             pltpu.VMEM((1, HEAD_SIZE), full),
             pltpu.VMEM(values.shape, half),
@@ -647,7 +685,7 @@
             pltpu.VMEM((nsp, cap, width), half),
             pltpu.VMEM((nsp, cap, width), half),
             pltpu.VMEM((nsp, cap, width), half),
-            dma((13,)),
+            dma((15,)),
             dma((nsp // 2,)),
             dma((nsp // 2,)),
             dma((nsp,)),
@@ -666,25 +704,29 @@
             dma((nsp,)),
         ],
         compiler_params=pltpu.CompilerParams(
-            collective_id=0, has_side_effects=True, vmem_limit_bytes=66_800_000
+            collective_id=0, has_side_effects=True, vmem_limit_bytes=40_000_000
         ),
     )(
-        cosine,
-        sine_a,
-        sine_b,
-        keys,
-        key_norm_gain[None, :],
-        values,
-        queries,
-        query_gain[None, :],
-        out_weight,
-        routes.T,
-        route_weight.T,
-        residual,
-        norm_gain[None, :],
-        expert_gate,
-        expert_up,
-        expert_down,
+        *map(
+            pinned,
+            (
+                by_row,
+                by_column,
+                keys,
+                key_norm_gain[None, :],
+                values,
+                queries,
+                query_gain[None, :],
+                out_weight,
+                routes.T,
+                route_weight.T,
+                residual,
+                norm_gain[None, :],
+                expert_gate,
+                expert_up,
+                expert_down,
+            ),
+        )
     )
 
 

time: 67.9 us -> 64.3 us (0.947)
  Pallas kernels: 65 us -> 63.5 us
  other arithmetic: 1.14 us -> 0 us
  local copies, waits for them, and re-layouts: 1.57 us -> 0.66 us
    pallas_call x1, Pallas kernels: 65 us -> 63.5 us  [on_device_fused(): pl.pallas_call(functools.partial(layer_kernel, (nsp, ntp, heads, cap, row...]
    select_n x1 -> x0, other arithmetic: 1.02 us -> none  [on_device_fused(): sine_b = jnp.where(first, 0.0, sine)]
    unnamed x1, local copies, waits for them, and re-layouts: 1.57 us -> 0.66 us
where the time goes in v1:
time: 64.3 us; the launch traced here: 64.2 us
  Pallas kernels  63.5 us (99%)
  local copies, waits for them, and re-layouts  0.66 us (1%)
    pallas_call x1, Pallas kernels, on_device_fused(): pl.pallas_call(functools.partial(layer_kernel, (nsp, ntp, heads, cap, row...  63.5 us

profile of v1, /device:TPU:0, one launch (start us, length us, event | category | flops | bytes accessed | tf_op | source)
XLA Modules:
  0.0 64.2 jit_solution(9525458224854016997)
XLA Ops:
  0.0 63.5 %shard_map.145 = bf16[32,2048]{1,0:T(8,128)(2,1)S(1)} custom-call(f32[8,2,256]{2,1,0:T(2,128)} %constant.4.clone.row_hbm, f32[64,256]{1,0:T(8,128)} %constant.5.clone.column_hbm, bf16[128,128]{1,0:T(8,128)(2,1)} %k_hbm.1, f32[1,128]{1,0:T(1,128)} %bitcast.8, bf16[128,128]{1,0:T(8,128)(2,1)} %v_hbm.1, bf16[128,512]{1,0:T(8,128)(2,1)} %q_hbm.1, ...), custom_call_target="tpu_custom_call" | custom-call | tf_op jit(solution)/shard_map/pallas_call | solution.py:649
  63.5 0.7 %copy.17 = bf16[32,2048]{1,0:T(8,128)(2,1)} copy(bf16[32,2048]{1,0:T(8,128)(2,1)S(1)} %shard_map.145) | data formatting | bytes 262144

commit v2 on v1

--- a/solution.py
+++ b/solution.py
@@ -171,6 +171,33 @@
 
 
 MESH = pl.DeviceIdType.MESH
+KV_ORDER = (1, 2, 4, 6)
+ORDER = (0, 1, 2, 4, 3, 5, 6, 7)
+O_GROUPS = ((0, 1, 2, 4), (3, 5, 6, 7))
+A_GROUPS = ((0, 1, 2, 4), (3, 5, 6, 7))
+LARGEST = 4
+LEAVING = (4, 1, 2, 5, 3, 6, 7)
+SCHEDULE = (
+    ("spread", (0, 1, 2, 4), ()),
+    ("weights", (), ()),
+    ("settle_mate", (0,), ()),
+    ("near", (0,), ((-1, "spread", (3, 5)),)),
+    ("forward", (0, 1, 2, 4), ()),
+    ("settle_diagonal", (0,), ()),
+    ("far", (0,), ((-1, "spread", (6,)),)),
+    ("spread", (7,), ()),
+    ("cross", (4, 2, 1, 0), ()),
+    ("settle_mate", (1,), ()),
+    ("near", (1,), ((-1, "forward", (3, 5, 6)),)),
+    ("forward", (7,), ()),
+    ("settle_diagonal", (1,), ()),
+    ("take", (0,), ()),
+    ("far", (1,), ((-1, "finish", (4,)),)),
+    ("cross", (7, 6, 5, 3), ()),
+    ("finish", (2, 1, 0), ()),
+    ("take", (1,), ()),
+    ("finish", (7, 6, 5, 3), ()),
+)
 LOG2E = 1.4426950408889634
 
 
@@ -196,7 +223,6 @@
     column_ref,
     k_ref,
     kgain_ref,
-    v_ref,
     q_ref,
     qgain_ref,
     routes_ref,
@@ -210,7 +236,10 @@
     wgate,
     wup,
     wdown,
-    kv,
+    k_all,
+    v_all,
+    probs,
+    sums,
     att,
     part,
     rs_in,
@@ -226,26 +255,22 @@
     outmail,
     back,
     wsem,
-    kv_send,
-    kv_fsend,
-    kv_recv,
-    rs_send,
+    gone,
+    send_sem,
+    k_recv,
+    v_recv,
     rs_recv,
-    mail_send,
-    x_send,
-    p_send,
-    f_send,
-    in_recv,
-    pair_send,
-    pair_recv,
-    rx_send,
+    mail_recv,
+    mate_recv,
+    x_recv,
+    diagonal_recv,
+    near_recv,
+    far_recv,
     rx_recv,
-    back_send,
     back_recv,
 ):
     nsp, ntp, heads, cap, rows, own_rows = dims
     width = out_ref.shape[1]
-    span = nsp // 2
     me = lax.axis_index("sp")
     tp = lax.axis_index("tp")
     far = me // 2
@@ -275,7 +300,7 @@
             (kgain_hbm, kgain_ref),
             (row_hbm.at[me], row_ref),
             (column_hbm, column_ref),
-            (v_hbm, kv.at[me, :, pl.ds(HEAD_SIZE, HEAD_SIZE)]),
+            (v_hbm, v_all.at[me]),
             (q_hbm, q_ref),
             (qgain_hbm, qgain_ref),
             (routes_hbm, routes_ref),
@@ -302,23 +327,22 @@
 
     sent = []
 
-    def push(source, target, send_sem, recv_sem, to_sp, to_tp):
-        copy = pltpu.make_async_remote_copy(
+    def push(source, target, recv_sem, to_sp, to_tp):
+        pltpu.make_async_remote_copy(
             src_ref=source,
             dst_ref=target,
-            send_sem=send_sem,
+            send_sem=send_sem.at[0],
             recv_sem=recv_sem,
             device_id=(to_sp, to_tp),
             device_id_type=MESH,
-        )
-        copy.start()
-        sent.append(copy)
-
-    def arrived(target, send_sem, recv_sem):
+        ).start()
+        sent.append(math.prod(source.shape))
+
+    def arrived(target, recv_sem):
         pltpu.make_async_remote_copy(
             src_ref=target,
             dst_ref=target,
-            send_sem=send_sem,
+            send_sem=send_sem.at[0],
             recv_sem=recv_sem,
             device_id=(twin, tp),
             device_id_type=MESH,
@@ -354,13 +378,33 @@
         loads[i].wait()
     sine = table(1)
     tables = (table(0), jnp.where(leading, -sine, 0.0), jnp.where(leading, 0.0, sine))
-    kv[me, :, :HEAD_SIZE] = turned(k_ref[...], kgain_ref, tables)
+    k_all[me] = turned(k_ref[...], kgain_ref, tables)
     loads[4].wait()
     pl.semaphore_wait(barrier, nsp - 1 + ntp - 1)
 
-    push(kv.at[me], kv.at[me], kv_send.at[0], kv_recv.at[me], twin, tp)
-    for d in range(1, span):
-        push(kv.at[me], kv.at[me], kv_send.at[d], kv_recv.at[me], peer(2 * d), tp)
+    key_side = (k_all, k_recv)
+    value_side = (v_all, v_recv)
+
+    def offer(side):
+        everyone, recv = side
+        for d in KV_ORDER:
+            arrival = recv.at[d // 2]
+            push(everyone.at[me], everyone.at[me], arrival, peer(d), tp)
+
+    def pass_on(side):
+        everyone, recv = side
+        for d in KV_ORDER:
+            if d > 1:
+                piece = everyone.at[peer(d)]
+                arrived(piece, recv.at[d // 2])
+                push(piece, piece, recv.at[0], twin, tp)
+
+    def complete(side):
+        everyone, recv = side
+        arrived(everyone.at[pl.ds(0, nsp // 2)], recv.at[0])
+
+    offer(key_side)
+    offer(value_side)
 
     loads[5].wait()
     loads[6].wait()
@@ -395,104 +439,134 @@
         wcol[j] = jnp.broadcast_to(column, wcol.shape[1:])
     placed_ref[...] = placer
 
-    for d in range(1, span):
-        source = peer(2 * d)
-        arrived(kv.at[source], kv_send.at[0], kv_recv.at[source])
-        push(kv.at[source], kv.at[source], kv_fsend.at[d], kv_recv.at[source], twin, tp)
-    for d in range(span):
-        source = peer(2 * d + 1)
-        arrived(kv.at[source], kv_send.at[0], kv_recv.at[source])
-
+    pass_on(key_side)
+    pass_on(value_side)
+    complete(key_side)
     scale = LOG2E / math.sqrt(HEAD_SIZE)
+    all_keys = k_all[...].reshape(nsp * rows, HEAD_SIZE)
     for h in range(heads):
-        columns = slice(h * HEAD_SIZE, (h + 1) * HEAD_SIZE)
-        all_keys = kv[:, :, :HEAD_SIZE].reshape(nsp * rows, HEAD_SIZE)
         scores = lax.dot_general(
-            att[:, columns],
+            att[:, h * HEAD_SIZE : (h + 1) * HEAD_SIZE],
             all_keys,
             (((1,), (1,)), ((), ())),
             preferred_element_type=jnp.float32,
         )
         top = jnp.max(scores, axis=-1, keepdims=True)
         weights = jnp.exp2((scores - top) * scale)
-        norm_sum = jnp.sum(weights, axis=-1, keepdims=True)
-        all_values = kv[:, :, HEAD_SIZE:].reshape(nsp * rows, HEAD_SIZE)
-        mixed = jnp.dot(
-            weights.astype(jnp.bfloat16), all_values, preferred_element_type=jnp.float32
-        )
-        att[:, columns] = (mixed / norm_sum).astype(jnp.bfloat16)
+        sums[h] = jnp.broadcast_to(jnp.sum(weights, axis=-1, keepdims=True), sums.shape[1:])
+        probs[h] = weights.astype(jnp.bfloat16)
+    complete(value_side)
+    all_values = v_all[...].reshape(nsp * rows, HEAD_SIZE)
+    for h in range(heads):
+        mixed = jnp.dot(probs[h], all_values, preferred_element_type=jnp.float32)
+        att[:, h * HEAD_SIZE : (h + 1) * HEAD_SIZE] = (mixed / sums[h]).astype(jnp.bfloat16)
 
     loads[11].wait()
     tile = 512
-
-    @pl.loop(0, width // tile)
-    def _(j):
-        columns = pl.ds(pl.multiple_of(j * tile, tile), tile)
+    tiles = width // tile
+
+    def tile_of(j):
+        return pl.ds(j * tile, tile)
+
+    strips = 2
+    strip_width = width // strips
+
+    def strip_of(j):
+        return pl.ds(j * strip_width, strip_width)
+
+    for j in range(tiles):
+        columns = slice(j * tile, (j + 1) * tile)
         product = jnp.dot(att[...], wout[:, columns], preferred_element_type=jnp.float32)
         part[:, :, columns] = product.astype(jnp.bfloat16).reshape(ntp, own_rows, tile)
-
-    push(part.at[diagonal], rs_in.at[1], rs_send.at[1], rs_recv.at[1], me, mate)
-    push(part.at[mate], rs_in.at[2], rs_send.at[2], rs_recv.at[2], me, mate)
-    arrived(rs_in.at[1], rs_send.at[1], rs_recv.at[1])
-    part[across] = (
-        part[across].astype(jnp.float32) + rs_in[1].astype(jnp.float32)
-    ).astype(jnp.bfloat16)
-    push(part.at[across], rs_in.at[3], rs_send.at[3], rs_recv.at[3], me, across)
+        if (j + 1) % (tiles // strips) == 0:
+            i = j // (tiles // strips)
+            push(
+                part.at[diagonal, :, strip_of(i)],
+                rs_in.at[1, :, strip_of(i)],
+                rs_recv.at[1 + i],
+                me,
+                mate,
+            )
+    push(part.at[mate], rs_in.at[2], rs_recv.at[0], me, mate)
+    for j in range(strips):
+        columns = slice(j * strip_width, (j + 1) * strip_width)
+        arrived(rs_in.at[1, :, strip_of(j)], rs_recv.at[1 + j])
+        part[across, :, columns] = (
+            part[across, :, columns].astype(jnp.float32)
+            + rs_in[1, :, columns].astype(jnp.float32)
+        ).astype(jnp.bfloat16)
+        push(
+            part.at[across, :, strip_of(j)],
+            rs_in.at[3, :, strip_of(j)],
+            rs_recv.at[1 + strips + j],
+            me,
+            across,
+        )
     loads[9].wait()
     loads[10].wait()
-    total = resid_ref[...].astype(jnp.float32) + part[tp].astype(jnp.float32)
-    for d in (2, 3):
-        arrived(rs_in.at[d], rs_send.at[d], rs_recv.at[d])
-        total = total + rs_in[d].astype(jnp.float32)
-    state[...] = total
-    normed = (
-        total
-        * lax.rsqrt(jnp.mean(total * total, axis=-1, keepdims=True) + norm_eps)
-        * ngain_ref[...]
-    ).astype(jnp.bfloat16)
+    arrived(rs_in.at[2], rs_recv.at[0])
+    squares = jnp.zeros((own_rows, 1), jnp.float32)
+    for j in range(strips):
+        columns = slice(j * strip_width, (j + 1) * strip_width)
+        early = (
+            resid_ref[:, columns].astype(jnp.float32)
+            + part[tp, :, columns].astype(jnp.float32)
+            + rs_in[2, :, columns].astype(jnp.float32)
+        )
+        arrived(rs_in.at[3, :, strip_of(j)], rs_recv.at[1 + strips + j])
+        total = early + rs_in[3, :, columns].astype(jnp.float32)
+        squares = squares + jnp.sum(total * total, axis=-1, keepdims=True)
+        state[:, columns] = total
+    normed = (state[...] * lax.rsqrt(squares / width + norm_eps) * ngain_ref[...]).astype(
+        jnp.bfloat16
+    )
     mail[...] = (
         jnp.dot(placed_ref[...], normed, preferred_element_type=jnp.float32)
         .astype(jnp.bfloat16)
         .reshape(nsp, cap, width)
     )
-    half = nsp // 2
-    quarter = nsp // 4
-    first = [*range(quarter), *range(half, half + quarter)]
-    groups = (first, [d for d in range(nsp) if d not in first])
-    relay = groups[0] + groups[1]
-    leaving = sorted(first, reverse=True) + sorted(groups[1], reverse=True)
-    for d in leaving:
-        if d:
-            to = peer(d)
-            push(mail.at[to], inbox.at[tp, me], mail_send.at[d], in_recv.at[tp, me], to, tp)
+    for d in LEAVING:
+        to = peer(d)
+        push(mail.at[to], inbox.at[tp, me], mail_recv.at[d], to, tp)
     inbox[tp, me] = mail[me]
 
-    def wait_piece(owner, d):
-        source = peer(d)
-        arrived(inbox.at[owner, source], mail_send.at[0], in_recv.at[owner, source])
-
-    def spread(g):
-        for d in groups[g]:
+    def group_of(groups, d):
+        return next(g for g, group in enumerate(groups) if d in group)
+
+    def spread(*pieces):
+        for d in pieces:
+            piece = inbox.at[tp, peer(d)]
             if d:
-                wait_piece(tp, d)
-            piece = inbox.at[tp, peer(d)]
-            arrival = in_recv.at[tp, peer(d)]
-            push(piece, piece, x_send.at[d], arrival, me, across)
-            push(piece, piece, p_send.at[d], arrival, me, mate)
-
-    def forward(g):
-        for d in groups[g]:
-            wait_piece(across, d)
+                arrived(piece, mail_recv.at[d])
+            push(piece, piece, x_recv.at[d], me, across)
+            push(piece, piece, mate_recv.at[group_of(O_GROUPS, d)], me, mate)
+
+    def forward(*pieces):
+        for d in pieces:
             piece = inbox.at[across, peer(d)]
-            arrival = in_recv.at[across, peer(d)]
-            push(piece, piece, f_send.at[d], arrival, me, mate)
-        for d in groups[g]:
-            wait_piece(diagonal, d)
+            arrived(piece, x_recv.at[d])
+            push(piece, piece, diagonal_recv.at[group_of(A_GROUPS, d)], me, mate)
+
+    def settle_mate(g):
+        arrived(inbox.at[mate, pl.ds(0, len(O_GROUPS[g]))], mate_recv.at[g])
+
+    def settle_diagonal(g):
+        arrived(inbox.at[diagonal, pl.ds(0, len(A_GROUPS[g]))], diagonal_recv.at[g])
+
+    def runs_of(pieces):
+        slots = sorted(ORDER.index(d) for d in pieces)
+        starts = [slot for slot in slots if slot - 1 not in slots]
+        ends = [slot + 1 for slot in slots if slot + 1 not in slots]
+        return list(zip(starts, ends))
+
+    def in_order(pieces):
+        return sorted(pieces, key=ORDER.index)
 
     fine = 256
 
-    def experts(parts):
-        blocks = [(owner, peer(d)) for owner, _, g in parts for d in groups[g]]
+    def experts(parts, pieces, hooks):
+        pieces = in_order(pieces)
+        blocks = [(owner, peer(d)) for owner, _ in parts for d in pieces]
         live = len(blocks) * cap
 
         @pl.loop(0, wgate.shape[1] // fine)
@@ -503,101 +577,137 @@
             up = jnp.dot(block, wup[:, columns], preferred_element_type=jnp.float32)
             hidden[:live, columns] = (gate / (1.0 + jnp.exp(-gate)) * up).astype(jnp.bfloat16)
 
-        @pl.loop(0, width // tile)
-        def _(j):
-            columns = pl.ds(pl.multiple_of(j * tile, tile), tile)
+        hooks(-1)
+        for j in range(tiles):
+            columns = slice(j * tile, (j + 1) * tile)
             product = jnp.dot(hidden[:live], wdown[:, columns], preferred_element_type=jnp.float32)
-            product = product.reshape(len(parts), half, cap, tile)
-            for i, (_, target, g) in enumerate(parts):
-                target[g * half : (g + 1) * half, :, columns] = product[i].astype(target.dtype)
-
-    def hand(i, g):
-        span_of = pl.ds(g * half, half)
-        k = 2 * i + g
-        push(
-            pair_out.at[i, span_of],
-            pair_in.at[i, span_of],
-            pair_send.at[k],
-            pair_recv.at[k],
-            me,
-            mate,
-        )
-
-    def take(i, g):
-        span_of = pl.ds(g * half, half)
-        k = 2 * i + g
-        arrived(pair_in.at[i, span_of], pair_send.at[k], pair_recv.at[k])
-
-    def cross(g):
-        take(1, g)
-        for d in sorted(groups[g], reverse=True):
-            slot = g * half + groups[g].index(d)
-            source = peer(d)
-            xsum[source] = (keep[1, slot] + pair_in[1, slot].astype(jnp.float32)).astype(
+            product = product.reshape(len(parts), len(pieces), cap, tile)
+            for i, (_, target) in enumerate(parts):
+                done = 0
+                for start, end in runs_of(pieces):
+                    count = end - start
+                    target[start:end, :, columns] = product[i, done : done + count].astype(
+                        target.dtype
+                    )
+                    done += count
+            hooks(j)
+
+    def strip(ref, start, end, j):
+        return ref.at[pl.ds(start, end - start), :, tile_of(j)]
+
+    def hand(i, pieces, arrival, j):
+        for start, end in runs_of(pieces):
+            push(
+                strip(pair_out.at[i], start, end, j),
+                strip(pair_in.at[i], start, end, j),
+                arrival,
+                me,
+                mate,
+            )
+
+    def take(i, pieces, arrival):
+        arrived(pair_in.at[i, pl.ds(0, len(pieces))], arrival)
+
+    def near_side(g, hooks):
+        pieces = O_GROUPS[g]
+
+        def each(j):
+            if j >= 0:
+                hand(0, pieces, near_recv.at[g], j)
+            hooks(j)
+
+        experts([(tp, keep.at[0]), (mate, pair_out.at[0])], pieces, each)
+
+    def far_side(g, hooks):
+        pieces = A_GROUPS[g]
+
+        def each(j):
+            if j >= 0:
+                hand(1, pieces, far_recv.at[g], j)
+            hooks(j)
+
+        experts([(diagonal, pair_out.at[1]), (across, keep.at[1])], pieces, each)
+
+    def cross(*order):
+        g = group_of(A_GROUPS, order[0])
+        take(1, A_GROUPS[g], far_recv.at[g])
+        for d in order:
+            slot = ORDER.index(d)
+            xsum[slot] = (keep[1, slot] + pair_in[1, slot].astype(jnp.float32)).astype(
                 jnp.bfloat16
             )
-            push(
-                xsum.at[source], xin.at[source], rx_send.at[d], rx_recv.at[source], me, across
+            push(xsum.at[slot], xin.at[slot], rx_recv.at[slot], me, across)
+
+    def finish(*pieces):
+        for d in pieces:
+            slot = ORDER.index(d)
+            source = peer(d)
+            arrived(xin.at[slot], rx_recv.at[slot])
+            summed = (
+                keep[0, slot]
+                + pair_in[0, slot].astype(jnp.float32)
+                + xin[slot].astype(jnp.float32)
+            ).astype(jnp.bfloat16)
+            if d:
+                outmail[slot] = summed
+                push(outmail.at[slot], back.at[me], back_recv.at[0], source, tp)
+            else:
+                back[me] = summed
+
+    def plan(steps):
+        table = {}
+        for at, action in steps:
+            table.setdefault(at, []).append(action)
+
+        def run(j):
+            for action in table.get(j, ()):
+                action()
+
+        return run
+
+    def later(function, *given):
+        return lambda: function(*given)
+
+    def weights_here():
+        for i in (12, 13, 14):
+            loads[i].wait()
+
+    simple = {
+        "spread": spread,
+        "forward": forward,
+        "finish": finish,
+        "settle_mate": settle_mate,
+        "settle_diagonal": settle_diagonal,
+        "weights": weights_here,
+        "cross": cross,
+        "take": lambda g: take(0, O_GROUPS[g], near_recv.at[g]),
+    }
+    for kind, given, hooks in SCHEDULE:
+        if kind in simple:
+            simple[kind](*given)
+            continue
+        run = plan([(at, later(simple[what], *pieces)) for at, what, pieces in hooks])
+        (near_side if kind == "near" else far_side)(*given, run)
+    arrived(back.at[pl.ds(0, nsp - 1)], back_recv.at[0])
+    for j in range(tiles):
+        columns = slice(j * tile, (j + 1) * tile)
+        returned = back[:, :, columns].reshape(nsp * cap, tile)
+        result = state[:, columns]
+        for i in range(picks.shape[0]):
+            chosen = lax.dot_general(
+                picks[i], returned, (((0,), (0,)), ((), ())), preferred_element_type=jnp.float32
             )
-
-    spread(0)
-    for i in (12, 13, 14):
-        loads[i].wait()
-    for d in groups[0]:
-        wait_piece(mate, d)
-    experts([(tp, keep.at[0], 0), (mate, pair_out.at[0], 0)])
-    hand(0, 0)
-    spread(1)
-    forward(0)
-    experts([(diagonal, pair_out.at[1], 0), (across, keep.at[1], 0)])
-    hand(1, 0)
-    cross(0)
-    for d in groups[1]:
-        wait_piece(mate, d)
-    forward(1)
-    experts(
-        [
-            (diagonal, pair_out.at[1], 1),
-            (across, keep.at[1], 1),
-            (tp, keep.at[0], 1),
-            (mate, pair_out.at[0], 1),
-        ]
-    )
-    hand(1, 1)
-    hand(0, 1)
-    cross(1)
-    for d in leaving:
-        g = 0 if d in first else 1
-        slot = g * half + groups[g].index(d)
-        source = peer(d)
-        if d == leaving[g * half]:
-            take(0, g)
-        arrived(xin.at[source], rx_send.at[0], rx_recv.at[source])
-        summed = (
-            keep[0, slot]
-            + pair_in[0, slot].astype(jnp.float32)
-            + xin[source].astype(jnp.float32)
-        ).astype(jnp.bfloat16)
-        if d:
-            outmail[source] = summed
-            push(
-                outmail.at[source], back.at[me], back_send.at[d], back_recv.at[me], source, tp
-            )
-        else:
-            back[me] = summed
-    for d in range(1, nsp):
-        source = peer(d)
-        arrived(back.at[source], back_send.at[0], back_recv.at[source])
-    returned = back[...].reshape(nsp * cap, width)
-    result = state[...]
-    for j in range(picks.shape[0]):
-        chosen = lax.dot_general(
-            picks[j], returned, (((0,), (0,)), ((), ())), preferred_element_type=jnp.float32
-        )
-        result = result + wcol[j, :, 0:1] * chosen
-    out_ref[...] = result.astype(out_ref.dtype)
-    for copy in sent:
-        copy.wait_send()
+            result = result + wcol[i, :, 0:1] * chosen
+        out_ref[:, columns] = result.astype(out_ref.dtype)
+    assert sum(sent) == math.prod(gone.shape)
+    pltpu.make_async_remote_copy(
+        src_ref=gone,
+        dst_ref=gone,
+        send_sem=send_sem.at[0],
+        recv_sem=back_recv.at[0],
+        device_id=(twin, tp),
+        device_id_type=MESH,
+    ).wait_send()
 
 
 def pinned(array):
@@ -616,6 +726,11 @@
 
     lines = rows // GRID_W
     return both(nsp * lines).reshape(nsp, lines, 2 * HEAD_SIZE), both(GRID_W)
+
+
+def sent_rows(nsp, ntp, rows, own_rows, cap, width):
+    attention = 2 * (nsp - 1) * rows * HEAD_SIZE // width
+    return attention + (ntp - 1) * own_rows + (2 * (nsp - 1) + 6 * nsp) * cap
 
 
 def on_device_fused(
@@ -656,7 +771,6 @@
             pltpu.VMEM(by_column.shape, full),
             pltpu.VMEM(keys.shape, half),
             pltpu.VMEM((1, HEAD_SIZE), full),
-            pltpu.VMEM(values.shape, half),
             pltpu.VMEM(queries.shape, half),
             pltpu.VMEM((1, HEAD_SIZE), full),
             pltpu.VMEM((top, own_rows), jnp.int32),
@@ -670,14 +784,17 @@
             pltpu.VMEM(expert_gate.shape[1:], half),
             pltpu.VMEM(expert_up.shape[1:], half),
             pltpu.VMEM(expert_down.shape[1:], half),
-            pltpu.VMEM((nsp, rows, 2 * HEAD_SIZE), half),
+            pltpu.VMEM((nsp, rows, HEAD_SIZE), half),
+            pltpu.VMEM((nsp, rows, HEAD_SIZE), half),
+            pltpu.VMEM((heads, rows, nsp * rows), half),
+            pltpu.VMEM((heads, rows, HEAD_SIZE), full),
             pltpu.VMEM(queries.shape, half),
             pltpu.VMEM((ntp, own_rows, width), half),
             pltpu.VMEM((ntp, own_rows, width), half),
             pltpu.VMEM((own_rows, width), full),
             pltpu.VMEM((nsp, cap, width), half),
             pltpu.VMEM((ntp, nsp, cap, width), half),
-            pltpu.VMEM((2 * nsp * cap, hidden_units), half),
+            pltpu.VMEM((2 * LARGEST * cap, hidden_units), half),
             pltpu.VMEM((2, nsp, cap, width), full),
             pltpu.VMEM((2, nsp, cap, width), half),
             pltpu.VMEM((2, nsp, cap, width), half),
@@ -686,22 +803,19 @@
             pltpu.VMEM((nsp, cap, width), half),
             pltpu.VMEM((nsp, cap, width), half),
             dma((15,)),
+            pltpu.VMEM((sent_rows(nsp, ntp, rows, own_rows, cap, width), width), half),
+            dma((1,)),
             dma((nsp // 2,)),
             dma((nsp // 2,)),
+            dma((5,)),
             dma((nsp,)),
-            dma((ntp,)),
-            dma((ntp,)),
+            dma((len(O_GROUPS),)),
             dma((nsp,)),
+            dma((len(A_GROUPS),)),
+            dma((len(O_GROUPS),)),
+            dma((len(A_GROUPS),)),
             dma((nsp,)),
-            dma((nsp,)),
-            dma((nsp,)),
-            dma((ntp, nsp)),
-            dma((4,)),
-            dma((4,)),
-            dma((nsp,)),
-            dma((nsp,)),
-            dma((nsp,)),
-            dma((nsp,)),
+            dma((1,)),
         ],
         compiler_params=pltpu.CompilerParams(
             collective_id=0, has_side_effects=True, vmem_limit_bytes=40_000_000
@@ -731,7 +845,7 @@
 
 
 def fits_fused(mesh):
-    return mesh.shape["tp"] == 4 and mesh.shape["sp"] in (4, 8)
+    return mesh.shape["tp"] == 4 and mesh.shape["sp"] == 8
 
 
 def solution(mesh):

time: 64.3 us -> 60 us (0.933)
  Pallas kernels: 63.5 us -> 59.2 us
    pallas_call x1, Pallas kernels: 63.5 us -> 59.2 us  [on_device_fused(): pl.pallas_call(functools.partial(layer_kernel, (nsp, ntp, heads, cap, row...]
where the time goes in v2:
time: 60 us; the launch traced here: 59.9 us
  Pallas kernels  59.2 us (99%)
  local copies, waits for them, and re-layouts  0.66 us (1%)
    pallas_call x1, Pallas kernels, on_device_fused(): pl.pallas_call(functools.partial(layer_kernel, (nsp, ntp, heads, cap, row...  59.2 us

profile of v2, /device:TPU:0, one launch (start us, length us, event | category | flops | bytes accessed | tf_op | source)
XLA Modules:
  0.0 59.9 jit_solution(1544891252088021578)
XLA Ops:
  0.0 59.2 %shard_map.145 = bf16[32,2048]{1,0:T(8,128)(2,1)S(1)} custom-call(f32[8,2,256]{2,1,0:T(2,128)} %constant.4.clone.row_hbm, f32[64,256]{1,0:T(8,128)} %constant.5.clone.column_hbm, bf16[128,128]{1,0:T(8,128)(2,1)} %k_hbm.1, f32[1,128]{1,0:T(1,128)} %bitcast.8, bf16[128,128]{1,0:T(8,128)(2,1)} %v_hbm.1, bf16[128,512]{1,0:T(8,128)(2,1)} %q_hbm.1, ...), custom_call_target="tpu_custom_call" | custom-call | tf_op jit(solution)/shard_map/pallas_call | solution.py:764
  59.2 0.7 %copy.17 = bf16[32,2048]{1,0:T(8,128)(2,1)} copy(bf16[32,2048]{1,0:T(8,128)(2,1)S(1)} %shard_map.145) | data formatting | bytes 262144

commit v3 on v2

--- a/solution.py
+++ b/solution.py
@@ -171,32 +171,36 @@
 
 
 MESH = pl.DeviceIdType.MESH
-KV_ORDER = (1, 2, 4, 6)
+KV_ORDER = (4, 1, 2)
+KV_SLOT = {1: 0, 2: 1, 4: 2}
+KV_RELAY = ((4, (3, 2, 1)), (2, (1,)))
 ORDER = (0, 1, 2, 4, 3, 5, 6, 7)
 O_GROUPS = ((0, 1, 2, 4), (3, 5, 6, 7))
-A_GROUPS = ((0, 1, 2, 4), (3, 5, 6, 7))
+A_GROUPS = ((0, 1, 2, 4), (3, 5), (6, 7))
 LARGEST = 4
 LEAVING = (4, 1, 2, 5, 3, 6, 7)
 SCHEDULE = (
     ("spread", (0, 1, 2, 4), ()),
     ("weights", (), ()),
     ("settle_mate", (0,), ()),
-    ("near", (0,), ((-1, "spread", (3, 5)),)),
-    ("forward", (0, 1, 2, 4), ()),
+    ("near", (0,), ((-3, "forward", (0,)), (-2, "spread", (3,)), (-1, "forward", (1, 2)), (1, "spread", (5,)))),
+    ("forward", (4,), ()),
     ("settle_diagonal", (0,), ()),
-    ("far", (0,), ((-1, "spread", (6,)),)),
+    ("far", (0,), ((-2, "spread", (6,)), (-1, "forward", (3, 5)))),
     ("spread", (7,), ()),
-    ("cross", (4, 2, 1, 0), ()),
+    ("settle_diagonal", (1,), ()),
+    ("far", (1,), ((-2, "take_far", (0,)), (-2, "cross", (4, 2)), (2, "forward", (6,)))),
     ("settle_mate", (1,), ()),
-    ("near", (1,), ((-1, "forward", (3, 5, 6)),)),
-    ("forward", (7,), ()),
-    ("settle_diagonal", (1,), ()),
-    ("take", (0,), ()),
-    ("far", (1,), ((-1, "finish", (4,)),)),
-    ("cross", (7, 6, 5, 3), ()),
-    ("finish", (2, 1, 0), ()),
-    ("take", (1,), ()),
-    ("finish", (7, 6, 5, 3), ()),
+    ("near", (1,), ((-2, "take_far", (1,)), (-2, "cross", (5, 3)), (-1, "forward", (7,)))),
+    ("take_near", (0,), ()),
+    ("finish", (4,), ()),
+    ("settle_diagonal", (2,), ()),
+    ("far", (2,), ((-1, "finish", (2,)),)),
+    ("take_near", (1,), ()),
+    ("finish", (5,), ()),
+    ("take_far", (2,), ()),
+    ("cross", (7, 6, 1, 0), ()),
+    ("finish", (3, 7, 6, 1, 0), ()),
 )
 LOG2E = 1.4426950408889634
 
@@ -385,23 +389,24 @@
     key_side = (k_all, k_recv)
     value_side = (v_all, v_recv)
 
+    half = nsp // 2
+
     def offer(side):
         everyone, recv = side
         for d in KV_ORDER:
-            arrival = recv.at[d // 2]
-            push(everyone.at[me], everyone.at[me], arrival, peer(d), tp)
+            push(everyone.at[me], everyone.at[me], recv.at[KV_SLOT[d]], peer(d), tp)
 
     def pass_on(side):
         everyone, recv = side
-        for d in KV_ORDER:
-            if d > 1:
-                piece = everyone.at[peer(d)]
-                arrived(piece, recv.at[d // 2])
-                push(piece, piece, recv.at[0], twin, tp)
+        for d, onward in KV_RELAY:
+            piece = everyone.at[peer(d)]
+            arrived(piece, recv.at[KV_SLOT[d]])
+            for to in onward:
+                push(piece, piece, recv.at[0], peer(to), tp)
 
     def complete(side):
         everyone, recv = side
-        arrived(everyone.at[pl.ds(0, nsp // 2)], recv.at[0])
+        arrived(everyone.at[pl.ds(0, nsp - 1 - len(KV_RELAY))], recv.at[0])
 
     offer(key_side)
     offer(value_side)
@@ -569,15 +574,15 @@
         blocks = [(owner, peer(d)) for owner, _ in parts for d in pieces]
         live = len(blocks) * cap
 
-        @pl.loop(0, wgate.shape[1] // fine)
-        def _(j):
-            columns = pl.ds(pl.multiple_of(j * fine, fine), fine)
+        steps = wgate.shape[1] // fine
+        for j in range(steps):
+            columns = slice(j * fine, (j + 1) * fine)
             block = jnp.concatenate([inbox[owner, source] for owner, source in blocks], axis=0)
             gate = jnp.dot(block, wgate[:, columns], preferred_element_type=jnp.float32)
             up = jnp.dot(block, wup[:, columns], preferred_element_type=jnp.float32)
             hidden[:live, columns] = (gate / (1.0 + jnp.exp(-gate)) * up).astype(jnp.bfloat16)
-
-        hooks(-1)
+            hooks(j - steps)
+
         for j in range(tiles):
             columns = slice(j * tile, (j + 1) * tile)
             product = jnp.dot(hidden[:live], wdown[:, columns], preferred_element_type=jnp.float32)
@@ -629,8 +634,6 @@
         experts([(diagonal, pair_out.at[1]), (across, keep.at[1])], pieces, each)
 
     def cross(*order):
-        g = group_of(A_GROUPS, order[0])
-        take(1, A_GROUPS[g], far_recv.at[g])
         for d in order:
             slot = ORDER.index(d)
             xsum[slot] = (keep[1, slot] + pair_in[1, slot].astype(jnp.float32)).astype(
@@ -680,7 +683,8 @@
         "settle_diagonal": settle_diagonal,
         "weights": weights_here,
         "cross": cross,
-        "take": lambda g: take(0, O_GROUPS[g], near_recv.at[g]),
+        "take_near": lambda g: take(0, O_GROUPS[g], near_recv.at[g]),
+        "take_far": lambda g: take(1, A_GROUPS[g], far_recv.at[g]),
     }
     for kind, given, hooks in SCHEDULE:
         if kind in simple:
@@ -805,8 +809,8 @@
             dma((15,)),
             pltpu.VMEM((sent_rows(nsp, ntp, rows, own_rows, cap, width), width), half),
             dma((1,)),
-            dma((nsp // 2,)),
-            dma((nsp // 2,)),
+            dma((3,)),
+            dma((3,)),
             dma((5,)),
             dma((nsp,)),
             dma((len(O_GROUPS),)),

time: 60 us -> 56 us (0.933)
  Pallas kernels: 59.2 us -> 55.1 us
    pallas_call x1, Pallas kernels: 59.2 us -> 55.1 us  [on_device_fused(): pl.pallas_call(functools.partial(layer_kernel, (nsp, ntp, heads, cap, row...]
where the time goes in v3:
time: 56 us; the launch traced here: 55.8 us
  Pallas kernels  55.1 us (98%)
  local copies, waits for them, and re-layouts  0.66 us (1%)
    pallas_call x1, Pallas kernels, on_device_fused(): pl.pallas_call(functools.partial(layer_kernel, (nsp, ntp, heads, cap, row...  55.1 us

profile of v3, /device:TPU:0, one launch (start us, length us, event | category | flops | bytes accessed | tf_op | source)
XLA Modules:
  0.0 55.8 jit_solution(3168858740393295068)
XLA Ops:
  0.0 55.1 %shard_map.145 = bf16[32,2048]{1,0:T(8,128)(2,1)S(1)} custom-call(f32[8,2,256]{2,1,0:T(2,128)} %constant.4.clone.row_hbm, f32[64,256]{1,0:T(8,128)} %constant.5.clone.column_hbm, bf16[128,128]{1,0:T(8,128)(2,1)} %k_hbm.1, f32[1,128]{1,0:T(1,128)} %bitcast.8, bf16[128,128]{1,0:T(8,128)(2,1)} %v_hbm.1, bf16[128,512]{1,0:T(8,128)(2,1)} %q_hbm.1, ...), custom_call_target="tpu_custom_call" | custom-call | tf_op jit(solution)/shard_map/pallas_call | solution.py:768
  55.2 0.7 %copy.17 = bf16[32,2048]{1,0:T(8,128)(2,1)} copy(bf16[32,2048]{1,0:T(8,128)(2,1)S(1)} %shard_map.145) | data formatting | bytes 262144

commit v4 on v3

--- a/solution.py
+++ b/solution.py
@@ -198,9 +198,15 @@
     ("far", (2,), ((-1, "finish", (2,)),)),
     ("take_near", (1,), ()),
     ("finish", (5,), ()),
-    ("take_far", (2,), ()),
-    ("cross", (7, 6, 1, 0), ()),
-    ("finish", (3, 7, 6, 1, 0), ()),
+    ("take_half", (0,), ()),
+    ("cross_half", (0, 7, 6), ()),
+    ("take_half", (1,), ()),
+    ("cross_half", (1, 7, 6), ()),
+    ("cross", (1, 0), ()),
+    ("finish", (3,), ()),
+    ("finish_half", (0, 7, 6), ()),
+    ("finish_half", (1, 7, 6), ()),
+    ("finish", (1, 0), ()),
 )
 LOG2E = 1.4426950408889634
 
@@ -628,7 +634,8 @@
 
         def each(j):
             if j >= 0:
-                hand(1, pieces, far_recv.at[g], j)
+                later_half = pieces == A_GROUPS[-1] and 2 * j >= tiles
+                hand(1, pieces, far_recv.at[g + 1 if later_half else g], j)
             hooks(j)
 
         experts([(diagonal, pair_out.at[1]), (across, keep.at[1])], pieces, each)
@@ -640,6 +647,52 @@
                 jnp.bfloat16
             )
             push(xsum.at[slot], xin.at[slot], rx_recv.at[slot], me, across)
+
+    def half_columns(h):
+        return pl.ds(h * (width // 2), width // 2)
+
+    def half_arrival(d, h):
+        return rx_recv.at[nsp + A_GROUPS[-1].index(d) if h else ORDER.index(d)]
+
+    def take_half(h):
+        last = A_GROUPS[-1]
+        arrived(
+            pair_in.at[1, pl.ds(0, len(last)), :, half_columns(h)],
+            far_recv.at[len(A_GROUPS) - 1 + h],
+        )
+
+    def cross_half(h, *order):
+        columns = slice(h * (width // 2), (h + 1) * (width // 2))
+        for d in order:
+            slot = ORDER.index(d)
+            xsum[slot, :, columns] = (
+                keep[1, slot, :, columns] + pair_in[1, slot, :, columns].astype(jnp.float32)
+            ).astype(jnp.bfloat16)
+            push(
+                xsum.at[slot, :, half_columns(h)],
+                xin.at[slot, :, half_columns(h)],
+                half_arrival(d, h),
+                me,
+                across,
+            )
+
+    def finish_half(h, *pieces):
+        columns = slice(h * (width // 2), (h + 1) * (width // 2))
+        for d in pieces:
+            slot = ORDER.index(d)
+            arrived(xin.at[slot, :, half_columns(h)], half_arrival(d, h))
+            outmail[slot, :, columns] = (
+                keep[0, slot, :, columns]
+                + pair_in[0, slot, :, columns].astype(jnp.float32)
+                + xin[slot, :, columns].astype(jnp.float32)
+            ).astype(jnp.bfloat16)
+            push(
+                outmail.at[slot, :, half_columns(h)],
+                back.at[me, :, half_columns(h)],
+                back_recv.at[0],
+                peer(d),
+                tp,
+            )
 
     def finish(*pieces):
         for d in pieces:
@@ -679,6 +732,9 @@
         "spread": spread,
         "forward": forward,
         "finish": finish,
+        "take_half": take_half,
+        "cross_half": cross_half,
+        "finish_half": finish_half,
         "settle_mate": settle_mate,
         "settle_diagonal": settle_diagonal,
         "weights": weights_here,
@@ -817,8 +873,8 @@
             dma((nsp,)),
             dma((len(A_GROUPS),)),
             dma((len(O_GROUPS),)),
-            dma((len(A_GROUPS),)),
-            dma((nsp,)),
+            dma((len(A_GROUPS) + 1,)),
+            dma((nsp + len(A_GROUPS[-1]),)),
             dma((1,)),
         ],
         compiler_params=pltpu.CompilerParams(

time: 56 us -> 55.4 us (0.989)
  no operation moved by 1% of the time
where the time goes in v4:
time: 55.4 us; the launch traced here: 55.3 us
  Pallas kernels  54.6 us (99%)
  local copies, waits for them, and re-layouts  0.66 us (1%)
    pallas_call x1, Pallas kernels, on_device_fused(): pl.pallas_call(functools.partial(layer_kernel, (nsp, ntp, heads, cap, row...  54.6 us

profile of v4, /device:TPU:0, one launch (start us, length us, event | category | flops | bytes accessed | tf_op | source)
XLA Modules:
  0.0 55.3 jit_solution(9646374901154786642)
XLA Ops:
  0.0 54.6 %shard_map.145 = bf16[32,2048]{1,0:T(8,128)(2,1)S(1)} custom-call(f32[8,2,256]{2,1,0:T(2,128)} %constant.4.clone.row_hbm, f32[64,256]{1,0:T(8,128)} %constant.5.clone.column_hbm, bf16[128,128]{1,0:T(8,128)(2,1)} %k_hbm.1, f32[1,128]{1,0:T(1,128)} %bitcast.8, bf16[128,128]{1,0:T(8,128)(2,1)} %v_hbm.1, bf16[128,512]{1,0:T(8,128)(2,1)} %q_hbm.1, ...), custom_call_target="tpu_custom_call" | custom-call | tf_op jit(solution)/shard_map/pallas_call | solution.py:824
  54.6 0.7 %copy.17 = bf16[32,2048]{1,0:T(8,128)(2,1)} copy(bf16[32,2048]{1,0:T(8,128)(2,1)S(1)} %shard_map.145) | data formatting | bytes 262144
